TPU v7x, 32 devices: a whole 2x2x4 slice. The times are simulated.
32 devices in a mesh: sp: 8 (over z, x), tp: 4 (over y, core).
Axes of the slice: x: 2, y: 2, z: 4, core: 2. Of those that a mesh axis runs over, the one named last changes fastest.
Arguments:
- queries: bfloat16 [8192, 2048], P('sp', 'tp'), may hold values from -16 to 16
- key_rows: bfloat16 [8192, 512], P('sp', 'tp'), may hold values from -16 to 16
- value_rows: bfloat16 [8192, 512], P('sp', 'tp'), may hold values from -6 to 6
- doc_ids: int32 [8192], P('sp'), may hold values from 0 to 3, never falling along the last dimension, each value on 1 to 4096 neighbouring positions
- sink_logit: float32 [32], P('tp'), may hold values from 3 to 7
- residual: bfloat16 [8192, 2048], P(('sp', 'tp')), may hold values from -6 to 6
- out_weight: bfloat16 [2048, 2048], P('tp'), may hold values from -3.5 to 3.5
- norm_gain: float32 [2048], replicated, may hold values from 0.1 to 1.9
- gate_weight: bfloat16 [8, 2048, 512], P('sp'), may hold values from -0.125 to 0.125
- up_weight: bfloat16 [8, 2048, 512], P('sp'), may hold values from -0.125 to 0.125
- down_weight: bfloat16 [8, 512, 2048], P('sp'), may hold values from -0.25 to 0.25
- routes: int32 [8192, 2], P(('sp', 'tp')), may hold values from 0 to 7, as said below
- route_weights: float32 [8192, 2], P(('sp', 'tp')), may hold values from 0.2 to 0.8
Outputs:
- mixed: bfloat16 [8192, 2048], P(('sp', 'tp'))
Inputs may be any that keep to these rules, and one draw needn't show every extreme that they name: `doc_ids`: never falls along the positions. `routes`: each aligned block of 256 rows names every expert exactly 64 times; the experts of one row differ and lie in one group of 2 consecutive numbers.
All inputs are finite; a program needn't handle non-finite values.
Results may differ from a plain program's by a relative error of at most 0.012.
Values may be sent and summed in bfloat16 or wider, within the bound.
A program may use at most 128 MiB of HBM per device.

v0:
```python
import jax
import jax.numpy as jnp
from jax import lax
from jax.sharding import PartitionSpec as P

HD = 64
WINDOW = 128


neg_fill = -1e30
eps_norm = 1e-06


def extended(block, sides, width):
    for axis, dim in sides:
        count = lax.axis_size(axis)
        forward = [(i, i + 1) for i in range(count - 1)]
        backward = [(target, source) for source, target in forward]
        low = lax.ppermute(
            lax.slice_in_dim(block, block.shape[dim] - width, None, axis=dim), axis, forward
        )
        high = lax.ppermute(lax.slice_in_dim(block, 0, width, axis=dim), axis, backward)
        block = jnp.concatenate([low, block, high], axis=dim)
    return block


def attend(
    query_part,
    key_part,
    value_part,
    query_docs,
    key_docs,
    query_start,
    key_start,
    sink_logit,
    extent,
):
    query_count = query_part.shape[0]
    key_count = key_part.shape[0]
    groups = key_part.shape[1] // HD
    head_ratio = sink_logit.shape[0] // groups
    query_heads = query_part.reshape(query_count, groups, head_ratio, HD)
    key_heads = key_part.reshape(key_count, groups, HD)
    value_heads = value_part.reshape(key_count, groups, HD)
    scores = jnp.einsum(
        "qgrd,kgd->grqk", query_heads, key_heads, preferred_element_type=jnp.float32
    ) * HD ** (-0.5)
    query_pos = query_start + jnp.arange(query_count, dtype=jnp.int32)
    key_pos = key_start + jnp.arange(key_count, dtype=jnp.int32)
    inside = (key_pos >= 0) & (key_pos < extent)
    allowed = (
        (jnp.abs(query_pos[:, None] - key_pos[None, :]) <= WINDOW)
        & (query_docs[:, None] == key_docs[None, :])
        & inside[None, :]
    )
    masked = jnp.where(allowed[None, None], scores, neg_fill)
    sink_col = sink_logit.reshape(groups, head_ratio)[:, :, None, None]
    row_top = jnp.maximum(jnp.max(masked, axis=3, keepdims=True), sink_col)
    exponent = jnp.where(allowed[None, None], jnp.exp(masked - row_top), 0.0)
    denominator = jnp.sum(exponent, axis=3, keepdims=True) + jnp.exp(sink_col - row_top)
    attn_weight = (exponent / denominator).astype(jnp.bfloat16)
    attended = jnp.einsum(
        "grqk,kgd->qgrd", attn_weight, value_heads, preferred_element_type=jnp.float32
    )
    return attended.astype(jnp.bfloat16).reshape(query_count, -1)


def fetch_margins(key_rows, value_rows, doc_float):
    return (
        extended(key_rows, (("sp", 0),), WINDOW),
        extended(value_rows, (("sp", 0),), WINDOW),
        extended(doc_float, (("sp", 0),), WINDOW),
    )


def per_device(
    queries,
    key_rows,
    value_rows,
    doc_ids,
    sink_logit,
    residual,
    out_weight,
    norm_gain,
    gate_weight,
    up_weight,
    down_weight,
    routes,
    route_weights,
):
    local_rows = queries.shape[0]
    anchor = lax.axis_index("sp") * local_rows
    extent = local_rows * lax.axis_size("sp")
    doc_float = doc_ids.astype(jnp.bfloat16)
    block_rows = min(512, local_rows)
    padded_keys, padded_values, padded_docs = fetch_margins(key_rows, value_rows, doc_float)
    block_parts = []
    for row_start in range(0, local_rows, block_rows):
        key_end = row_start + block_rows + 2 * WINDOW
        block_parts.append(
            attend(
                queries[row_start : row_start + block_rows],
                padded_keys[row_start:key_end],
                padded_values[row_start:key_end],
                doc_float[row_start : row_start + block_rows],
                padded_docs[row_start:key_end],
                anchor + row_start,
                anchor + row_start - WINDOW,
                sink_logit,
                extent,
            )
        )
    attended = jnp.concatenate(block_parts, axis=0)
    regrouped = lax.all_to_all(attended, "tp", split_axis=0, concat_axis=1, tiled=True)
    shard_rows = out_weight.shape[0]
    initial = jnp.zeros((regrouped.shape[0], out_weight.shape[1]), jnp.float32)
    running = initial
    weight_piece = lax.all_gather(out_weight, "tp", axis=0, tiled=True)
    for shard_index in range(weight_piece.shape[0] // shard_rows):
        columns = lax.dynamic_slice_in_dim(regrouped, shard_index * shard_rows, shard_rows, 1)
        partial_value = jnp.dot(
            columns,
            weight_piece[shard_index * shard_rows : (shard_index + 1) * shard_rows],
            preferred_element_type=jnp.float32,
        )
        running = running + partial_value.astype(jnp.bfloat16).astype(jnp.float32)
    stream = (residual.astype(jnp.float32) + running).astype(jnp.bfloat16)
    stream_f = stream.astype(jnp.float32)
    scale = lax.rsqrt(jnp.mean(stream_f * stream_f, axis=1, keepdims=True) + eps_norm)
    normed = (stream_f * scale * norm_gain[None, :]).astype(jnp.bfloat16)
    home_rows = normed.shape[0]
    width = normed.shape[1]
    route_count = routes.shape[1]
    expert_count = lax.axis_size("sp") * gate_weight.shape[0]
    capacity = route_count * home_rows // expert_count
    flat_routes = routes.reshape(-1)
    one_hot = (flat_routes[:, None] == jnp.arange(expert_count, dtype=jnp.int32)[None, :]).astype(
        jnp.int32
    )
    earlier = jnp.cumsum(one_hot, axis=0) - one_hot
    slot_rank = jnp.sum(earlier * one_hot, axis=1)
    slot_index = flat_routes * capacity + slot_rank
    source_row = (
        jnp.zeros((expert_count * capacity,), jnp.int32)
        .at[slot_index]
        .set(jnp.arange(home_rows * route_count, dtype=jnp.int32) // route_count)
    )
    outgoing = normed[source_row].reshape(expert_count, capacity, width)
    incoming = lax.all_to_all(outgoing, "sp", split_axis=0, concat_axis=0, tiled=True)
    flat_rows = incoming.reshape(-1, width)
    gate_act = jnp.dot(flat_rows, gate_weight[0], preferred_element_type=jnp.float32)
    up_act = jnp.dot(flat_rows, up_weight[0], preferred_element_type=jnp.float32)
    hidden = (jax.nn.silu(gate_act) * up_act).astype(jnp.bfloat16)
    produced = jnp.dot(hidden, down_weight[0], preferred_element_type=jnp.float32).astype(
        jnp.bfloat16
    )
    returned = lax.all_to_all(
        produced.reshape(incoming.shape), "sp", split_axis=0, concat_axis=0, tiled=True
    )
    route_out = returned.reshape(-1, width)[slot_index].reshape(home_rows, route_count, width)
    weighted = jnp.sum(route_weights[:, :, None] * route_out.astype(jnp.float32), axis=1)
    return (stream_f + weighted).astype(jnp.bfloat16)


def solution(mesh):
    return jax.shard_map(
        per_device,
        mesh=mesh,
        in_specs=(
            P("sp", "tp"),
            P("sp", "tp"),
            P("sp", "tp"),
            P("sp"),
            P("tp"),
            P(("sp", "tp"), None),
            P("tp", None),
            P(),
            P("sp", None, None),
            P("sp", None, None),
            P("sp", None, None),
            P(("sp", "tp"), None),
            P(("sp", "tp"), None),
        ),
        out_specs=P(("sp", "tp"), None),
        check_vma=False,
    )
```

profile of v0, /device:TPU:0, one launch (start us, length us, event | category | flops | bytes accessed | tf_op | source)
XLA Modules:
  0.0 266.3 jit_solution(878454835703081858)
XLA Ops:
  8.0 4.9 %collective-permute-start.1 = (bf16[128]{0:T(256)(128)(2,1)S(1)}, bf16[128]{0:T(256)(128)(2,1)S(1)}, u32[]{:S(2)}, u32[]{:S(2)}) collective-permute-start(bf16[128]{0:T(256)(128)(2,1)S(1)} %get-tuple-element.17), channel_id=1, source_target_pairs={{0,4},{4,8},{8,12},{12,16},{16,20},{20,24},{24,28},{1,5},{5,9},{9,... | collective-permute-start | bytes 776 | tf_op jit(solution)/shard_map/ppermute | solution.py:19
  12.8 1.3 collective-permute-start.4
  14.1 1.4 fusion.63
  15.5 4.5 %collective-permute-start.2 = (bf16[128,128]{1,0:T(8,128)(2,1)}, bf16[128,128]{1,0:T(8,128)(2,1)S(1)}, u32[]{:S(2)}, u32[]{:S(2)}) collective-permute-start(bf16[128,128]{1,0:T(8,128)(2,1)} %get-tuple-element.9), channel_id=1, source_target_pairs={{0,4},{4,8},{8,12},{12,16},{16,20},{20,24},{24,28},{1,5},{5,9},{9,... | collective-permute-start | bytes 98312 | tf_op jit(solution)/shard_map/ppermute | solution.py:19
  20.1 1.3 collective-permute-start.5
  21.4 1.4 fusion.64
  22.8 5.0 %collective-permute-start = (bf16[128,128]{1,0:T(8,128)(2,1)}, bf16[128,128]{1,0:T(8,128)(2,1)S(1)}, u32[]{:S(2)}, u32[]{:S(2)}) collective-permute-start(bf16[128,128]{1,0:T(8,128)(2,1)} %get-tuple-element.13), channel_id=1, source_target_pairs={{0,4},{4,8},{8,12},{12,16},{16,20},{20,24},{24,28},{1,5},{5,9},{9,... | collective-permute-start | bytes 98312 | tf_op jit(solution)/shard_map/ppermute | solution.py:19
  28.8 1.3 fusion.62
  30.0 1.0 copy.37
  31.6 1.1 reduce-window.6
  37.1 1.0 copy.41
  39.5 1.3 collective-permute-start.3
  41.6 2.4 fusion.30
  44.0 1.8 pad_maximum_fusion.3
  45.7 1.7 copy.36
  47.5 1.7 copy.40
  49.2 1.8 pad_maximum_fusion.4
  51.0 1.7 copy.35
  52.8 3.1 %fusion = (f32[2,4,512]{2,1,0:T(4,128)S(1)}, f32[2,768,512,4]{2,1,3,0:T(8,128)S(1)}) fusion(pred[512,768]{0,1:T(8,128)(4,1)S(1)} %get-tuple-element.30, bf16[768,2,64,1]{0,2,3,1:T(8,128)(2,1)} %bitcast.107, bf16[512,2,4,64]{0,3,2,1:T(8,128)(2,1)S(1)} %bitcast.104), kind=kOutput, calls=%fused_computation.9 | convolution fusion | flops 412086272 | bytes 13713408 | tf_op jit(solution)/shard_map/qgrd,kgd->grqk/dot_general | solution.py:45
  55.9 6.6 %fusion.1 = (f32[2,4,512]{2,1,0:T(4,128)S(1)}, f32[2,768,512,4]{2,1,3,0:T(8,128)}) fusion(pred[512,768]{0,1:T(8,128)(4,1)S(1)} %get-tuple-element.29, bf16[768,2,64,1]{0,2,3,1:T(8,128)(2,1)S(1)} %bitcast.106, bf16[512,2,4,64]{0,3,2,1:T(8,128)(2,1)S(1)} %bitcast.105), kind=kOutput, calls=%fused_computation.10 | convolution fusion | flops 412086272 | bytes 13713408 | tf_op jit(solution)/shard_map/qgrd,kgd->grqk/dot_general | solution.py:45
  62.5 3.1 %fusion.2 = f32[2,4,512]{2,1,0:T(4,128)S(1)} fusion(f32[2,768,512,4]{2,1,3,0:T(8,128)S(1)} %get-tuple-element.24, f32[2,4,512]{2,1,0:T(4,128)S(1)} %broadcast_maximum_fusion.1, pred[512,768]{0,1:T(8,128)(4,1)S(1)} %get-tuple-element.30), kind=kLoop, calls=%fused_computation.11 | loop fusion | flops 15724544 | bytes 13008896 | tf_op jit(solution)/shard_map/reduce_sum | solution.py:60
  65.7 4.7 %fusion.39 = bf16[2,64,4,512]{3,1,2,0:T(8,128)(2,1)} fusion(bf16[768,2,64,1]{0,2,3,1:T(8,128)(2,1)S(1)} %bitcast.110, f32[2,768,512,4]{2,1,3,0:T(8,128)S(1)} %get-tuple-element.24, f32[2,4,512]{2,1,0:T(4,128)S(1)} %get-tuple-element.21, f32[2,4,512]{2,1,0:T(4,128)S(1)} %broadcast_maximum_fusion.1, pred[512,768]{0,1:T(8,128)(4,1)S(1)} %get-tuple-element.30), kind=kOutput, calls=%fused_computation.55 | convolution fusion | flops 421789696 | bytes 13729792 | tf_op jit(solution)/shard_map/grqk,kgd->qgrd/dot_general | solution.py:62
  70.4 1.3 copy.43
  71.8 6.8 %fusion.3 = f32[2,4,512]{2,1,0:T(4,128)S(1)} fusion(f32[2,768,512,4]{2,1,3,0:T(8,128)} %get-tuple-element.26, f32[2,4,512]{2,1,0:T(4,128)S(1)} %get-tuple-element.22, pred[512,768]{0,1:T(8,128)(4,1)S(1)} %get-tuple-element.29), kind=kLoop, calls=%fused_computation.12 | loop fusion | flops 15724544 | bytes 13008896 | tf_op jit(solution)/shard_map/reduce_sum | solution.py:60
  78.7 1.3 copy-done.1
  80.1 4.6 %fusion.38 = bf16[2,64,4,512]{3,1,2,0:T(8,128)(2,1)} fusion(bf16[768,2,64,1]{0,2,3,1:T(8,128)(2,1)S(1)} %bitcast.111, f32[2,768,512,4]{2,1,3,0:T(8,128)S(1)} %copy-done.1, f32[2,4,512]{2,1,0:T(4,128)S(1)} %exponential_add_fusion, f32[2,4,512]{2,1,0:T(4,128)S(1)} %get-tuple-element.22, pred[512,768]{0,1:T(8,128)(4,1)S(1)} %get-tuple-element.29), kind=kOutput, calls=%fused_computation.54 | convolution fusion | flops 421789696 | bytes 13729792 | tf_op jit(solution)/shard_map/grqk,kgd->qgrd/dot_general | solution.py:62
  84.7 1.3 copy.44
  86.0 1.0 pad_maximum_fusion
  87.0 3.8 %all-to-all-start = ((bf16[4,256,512]{2,1,0:T(8,128)(2,1)}), bf16[4,256,512]{2,1,0:T(8,128)(2,1)S(1)}, u32[]{:S(2)}, u32[]{:S(2)}) async-start(bf16[4,256,512]{2,1,0:T(8,128)(2,1)} %bitcast.100), calls=%async_computation | async-start | bytes 2097152 | tf_op jit(solution)/shard_map/all_to_all | solution.py:114
  91.0 2.4 scatter_custom_fusion
  93.4 11.6 %all-to-all-done = bf16[4,256,512]{2,1,0:T(8,128)(2,1)S(1)} async-done(((bf16[4,256,512]{2,1,0:T(8,128)(2,1)}), bf16[4,256,512]{2,1,0:T(8,128)(2,1)S(1)}, u32[]{:S(2)}, u32[]{:S(2)}) %all-to-all-start) | async-done | bytes 1048608 | tf_op jit(solution)/shard_map/all_to_all | solution.py:114
  105.1 1.0 copy-done.5
  106.0 1.5 copy.45
  107.5 2.5 fusion.12
  110.0 2.9 %fusion.13 = f32[256,2048]{1,0:T(8,128)S(1)} fusion(bf16[2048,2048]{1,0:T(8,128)(2,1)} %all-gather.2.cloned.1.call-done, bf16[256,2048]{0,1:T(8,128)(2,1)S(1)} %bitcast.96), kind=kOutput, calls=%fused_computation.31 | convolution fusion | flops 537919488 | bytes 4456448 | tf_op jit(solution)/shard_map/dot_general | solution.py:121
  114.1 1.2 fusion.15
  115.3 1.0 copy-done.2
  116.6 3.3 %gather_fusion = bf16[512,2048]{1,0:T(8,128)(2,1)} fusion(bf16[256,2048]{1,0:T(8,128)(2,1)S(1)} %fusion.17, s32[1024]{0:T(1024)S(1)} %pad_clamp_fusion.1), kind=kCustom, calls=%fused_computation | custom fusion | bytes 4196352 | tf_op jit(solution)/shard_map/gather | solution.py:148
  119.9 56.4 %all_to_all.29 = bf16[8,64,2048]{2,1,0:T(8,128)(2,1)S(1)} all-to-all(bf16[8,64,2048]{2,1,0:T(8,128)(2,1)} %bitcast.94), channel_id=1, replica_groups=mesh['sp'=8,'tp'=4] {'sp'}, dimensions={0} | all-to-all | bytes 4194304 | tf_op jit(solution)/shard_map/all_to_all | solution.py:149
  176.3 1.3 copy-done.6
  177.7 1.2 fusion.26
  178.9 6.0 %convolution_convert_fusion = bf16[512,2048]{1,0:T(8,128)(2,1)} fusion(bf16[1,512,2048]{2,1,0:T(8,128)(2,1)S(1)} %copy-done, bf16[512,2048]{1,0:T(8,128)(2,1)} %bitcast.103, bf16[1,2048,512]{2,1,0:T(8,128)(2,1)} %param.22, f32[512,512]{1,0:T(8,128)S(1)} %fusion.26), kind=kOutput, calls=%fused_computation.19 | convolution fusion | flops 2150105088 | bytes 9437184 | tf_op jit(solution)/shard_map/dot_general | solution.py:154
  184.9 4.7 %all-to-all-start.2 = ((bf16[8,64,2048]{2,1,0:T(8,128)(2,1)}), bf16[8,64,2048]{2,1,0:T(8,128)(2,1)}, u32[]{:S(2)}, u32[]{:S(2)}) async-start(bf16[8,64,2048]{2,1,0:T(8,128)(2,1)} %bitcast.101), calls=%async_computation.2 | async-start | bytes 4194304 | tf_op jit(solution)/shard_map/all_to_all | solution.py:157
  189.8 46.9 %all-to-all-done.2 = bf16[8,64,2048]{2,1,0:T(8,128)(2,1)} async-done(((bf16[8,64,2048]{2,1,0:T(8,128)(2,1)}), bf16[8,64,2048]{2,1,0:T(8,128)(2,1)}, u32[]{:S(2)}, u32[]{:S(2)}) %all-to-all-start.2) | async-done | bytes 2097184 | tf_op jit(solution)/shard_map/all_to_all | solution.py:157
  236.7 7.1 %gather_fusion.1 = bf16[512,2048]{1,0:T(8,128)(2,1)} fusion(bf16[512,2048]{1,0:T(8,128)(2,1)} %bitcast.33, s32[1024]{0:T(1024)S(1)} %pad_clamp_fusion), kind=kCustom, calls=%fused_computation.1 | custom fusion | bytes 4196352 | tf_op jit(solution)/shard_map/gather | solution.py:160
  243.8 5.4 %reshape.312 = f32[256,2,2048]{2,1,0:T(2,128)} reshape(bf16[512,2048]{1,0:T(8,128)(2,1)} %gather_fusion.1) | data formatting | bytes 6291456 | tf_op jit(solution)/shard_map/convert_element_type | solution.py:161
  249.2 9.0 %multiply_reduce_fusion = f32[256,2048]{1,0:T(8,128)S(1)} fusion(f32[256,2,2048]{2,1,0:T(2,128)} %reshape.312, f32[256,2]{1,0:T(8,128)S(1)} %copy.46), kind=kLoop, calls=%fused_computation.15 | loop fusion | flops 1572864 | bytes 6293504 | tf_op jit(solution)/shard_map/reduce_sum | solution.py:161
  258.2 1.3 fusion.18
  (91 shorter events, 11.7 us)
Async XLA Ops:
  6.5 172.4 %copy-start = (bf16[1,512,2048]{2,1,0:T(8,128)(2,1)S(1)}, bf16[1,512,2048]{2,1,0:T(8,128)(2,1)}, u32[]{:S(2)}) copy-start(bf16[1,512,2048]{2,1,0:T(8,128)(2,1)} %param.23) | copy-start | bytes 6291460
  6.5 0.8 copy-start.20
  6.5 21.2 %copy-start.18 = (s32[256,2]{0,1:T(2,128)S(1)}, s32[256,2]{0,1:T(2,128)}, u32[]{:S(2)}) copy-start(s32[256,2]{0,1:T(2,128)} %param.24) | copy-start | bytes 6148
  6.5 101.0 %all-gather.2.cloned.1.call-start = ((), (), s32[]{:S(2)}) async-start(), calls=%async_computation.3 | async-start | bytes 10485760 | tf_op jit(solution)/shard_map/all_gather | solution.py:118
  7.4 23.7 %copy-start.24 = (f32[8]{0:T(128)S(1)}, f32[8]{0:T(128)}, u32[]{:S(2)}) copy-start(f32[8]{0:T(128)} %param.17) | copy-start | bytes 100
  7.4 30.7 %copy-start.13 = (bf16[1024]{0:T(1024)(128)(2,1)}, bf16[1024]{0:T(1024)(128)(2,1)S(1)}, u32[]{:S(2)}) copy-start(bf16[1024]{0:T(1024)(128)(2,1)S(1)} %convert_element_type.80) | copy-start | bytes 6148
  8.0 31.1 %collective-permute-start.1 = (bf16[128]{0:T(256)(128)(2,1)S(1)}, bf16[128]{0:T(256)(128)(2,1)S(1)}, u32[]{:S(2)}, u32[]{:S(2)}) collective-permute-start(bf16[128]{0:T(256)(128)(2,1)S(1)} %get-tuple-element.17), channel_id=1, source_target_pairs={{0,4},{4,8},{8,12},{12,16},{16,20},{20,24},{24,28},{1,5},{5,9},{9,... | collective-permute-start | bytes 776 | tf_op jit(solution)/shard_map/ppermute | solution.py:19
  12.8 28.0 %collective-permute-start.4 = (bf16[128]{0:T(256)(128)(2,1)}, bf16[128]{0:T(256)(128)(2,1)}, u32[]{:S(2)}, u32[]{:S(2)}) collective-permute-start(bf16[128]{0:T(256)(128)(2,1)} %get-tuple-element.18), channel_id=1, source_target_pairs={{4,0},{8,4},{12,8},{16,12},{20,16},{24,20},{28,24},{5,1},{9,5},{13... | collective-permute-start | bytes 776 | tf_op jit(solution)/shard_map/ppermute | solution.py:22
  15.5 28.4 %collective-permute-start.2 = (bf16[128,128]{1,0:T(8,128)(2,1)}, bf16[128,128]{1,0:T(8,128)(2,1)S(1)}, u32[]{:S(2)}, u32[]{:S(2)}) collective-permute-start(bf16[128,128]{1,0:T(8,128)(2,1)} %get-tuple-element.9), channel_id=1, source_target_pairs={{0,4},{4,8},{8,12},{12,16},{16,20},{20,24},{24,28},{1,5},{5,9},{9,... | collective-permute-start | bytes 98312 | tf_op jit(solution)/shard_map/ppermute | solution.py:19
  20.1 23.9 %collective-permute-start.5 = (bf16[128,128]{1,0:T(8,128)(2,1)}, bf16[128,128]{1,0:T(8,128)(2,1)S(1)}, u32[]{:S(2)}, u32[]{:S(2)}) collective-permute-start(bf16[128,128]{1,0:T(8,128)(2,1)} %get-tuple-element.10), channel_id=1, source_target_pairs={{4,0},{8,4},{12,8},{16,12},{20,16},{24,20},{28,24},{5,1},{9,5},{13... | collective-permute-start | bytes 98312 | tf_op jit(solution)/shard_map/ppermute | solution.py:22
  22.8 26.5 %collective-permute-start = (bf16[128,128]{1,0:T(8,128)(2,1)}, bf16[128,128]{1,0:T(8,128)(2,1)S(1)}, u32[]{:S(2)}, u32[]{:S(2)}) collective-permute-start(bf16[128,128]{1,0:T(8,128)(2,1)} %get-tuple-element.13), channel_id=1, source_target_pairs={{0,4},{4,8},{8,12},{12,16},{16,20},{20,24},{24,28},{1,5},{5,9},{9,... | collective-permute-start | bytes 98312 | tf_op jit(solution)/shard_map/ppermute | solution.py:19
  38.1 14.7 %copy-start.7 = (bf16[512,512]{0,1:T(8,128)(2,1)S(1)}, bf16[512,512]{0,1:T(8,128)(2,1)}, u32[]{:S(2)}) copy-start(bf16[512,512]{0,1:T(8,128)(2,1)} %copy.37) | copy-start | bytes 1572868
  38.1 0.9 copy-start.14
  39.0 0.5 copy-start.22
  39.5 9.7 %collective-permute-start.3 = (bf16[128,128]{1,0:T(8,128)(2,1)}, bf16[128,128]{1,0:T(8,128)(2,1)S(1)}, u32[]{:S(2)}, u32[]{:S(2)}) collective-permute-start(bf16[128,128]{1,0:T(8,128)(2,1)} %get-tuple-element.14), channel_id=1, source_target_pairs={{4,0},{8,4},{12,8},{16,12},{20,16},{24,20},{28,24},{5,1},{9,5},{13... | collective-permute-start | bytes 98312 | tf_op jit(solution)/shard_map/ppermute | solution.py:22
  52.8 3.1 %copy-start.15 = (f32[2,4]{1,0:T(2,128)S(1)}, f32[2,4]{1,0:T(2,128)}, u32[]{:S(2)}) copy-start(f32[2,4]{1,0:T(2,128)} %max.32) | copy-start | bytes 100
  52.8 3.2 %copy-start.8 = (bf16[512,512]{0,1:T(8,128)(2,1)S(1)}, bf16[512,512]{0,1:T(8,128)(2,1)}, u32[]{:S(2)}) copy-start(bf16[512,512]{0,1:T(8,128)(2,1)} %copy.41) | copy-start | bytes 1572868
  52.8 3.2 %copy-start.11 = (bf16[768,128]{0,1:T(8,128)(2,1)S(1)}, bf16[768,128]{0,1:T(8,128)(2,1)}, u32[]{:S(2)}) copy-start(bf16[768,128]{0,1:T(8,128)(2,1)} %copy.40) | copy-start | bytes 589828
  62.5 3.2 %copy-start.12 = (bf16[768,128]{0,1:T(8,128)(2,1)S(1)}, bf16[768,128]{0,1:T(8,128)(2,1)}, u32[]{:S(2)}) copy-start(bf16[768,128]{0,1:T(8,128)(2,1)} %copy.35) | copy-start | bytes 589828
  65.7 5.9 %copy-start.10 = (bf16[768,128]{1,0:T(8,128)(2,1)S(1)}, bf16[768,128]{1,0:T(8,128)(2,1)}, u32[]{:S(2)}) copy-start(bf16[768,128]{1,0:T(8,128)(2,1)} %get-tuple-element.12) | copy-start | bytes 589828
  71.8 8.2 %copy-start.1 = (f32[2,768,512,4]{2,1,3,0:T(8,128)S(1)}, f32[2,768,512,4]{2,1,3,0:T(8,128)}, u32[]{:S(2)}) copy-start(f32[2,768,512,4]{2,1,3,0:T(8,128)} %get-tuple-element.26) | copy-start | bytes 37748740
  87.0 3.9 %slice-start = ((s32[8,5]{0,1:T(8,128)}), s32[8,4]{0,1:T(4,128)S(1)}, s32[]{:S(2)}) async-start(s32[8,5]{0,1:T(8,128)} %copy-done.14), calls=%async_computation.4 | async-start | bytes 4096 | tf_op jit(solution)/shard_map/slice.1
  87.0 3.9 %copy-start.19 = (s32[512]{0:T(512)S(1)}, s32[512]{0:T(512)}, u32[]{:S(2)}) copy-start(s32[512]{0:T(512)} %eq.65) | copy-start | bytes 6148
  87.0 4.0 %copy-start.17 = (s32[512,1]{0,1:T(1,128)S(1)}, s32[512,1]{0,1:T(1,128)}, u32[]{:S(2)}) copy-start(s32[512,1]{0,1:T(1,128)} %mul.81) | copy-start | bytes 6148
  87.0 18.1 %all-to-all-start = ((bf16[4,256,512]{2,1,0:T(8,128)(2,1)}), bf16[4,256,512]{2,1,0:T(8,128)(2,1)S(1)}, u32[]{:S(2)}, u32[]{:S(2)}) async-start(bf16[4,256,512]{2,1,0:T(8,128)(2,1)} %bitcast.100), calls=%async_computation | async-start | bytes 2097152 | tf_op jit(solution)/shard_map/all_to_all | solution.py:114
  105.1 1.0 copy-start.5
  107.5 5.3 %copy-start.4 = (bf16[2048,2048]{1,0:T(8,128)(2,1)S(1)}, bf16[2048,2048]{1,0:T(8,128)(2,1)}, u32[]{:S(2)}) copy-start(bf16[2048,2048]{1,0:T(8,128)(2,1)} %all-gather.2.cloned.1.call-done) | copy-start | bytes 25165828
  112.9 1.2 copy-start.9
  114.1 2.2 copy-start.16
  115.3 1.0 copy-start.2
  119.9 57.8 %copy-start.23 = (bf16[1,2048,512]{2,1,0:T(8,128)(2,1)S(1)}, bf16[1,2048,512]{2,1,0:T(8,128)(2,1)}, u32[]{:S(2)}) copy-start(bf16[1,2048,512]{2,1,0:T(8,128)(2,1)} %param.21) | copy-start | bytes 6291460
  176.3 1.3 copy-start.6
  184.9 4.7 %copy-start.21 = (f32[256,2]{0,1:T(2,128)S(1)}, f32[256,2]{0,1:T(2,128)}, u32[]{:S(2)}) copy-start(f32[256,2]{0,1:T(2,128)} %param.25) | copy-start | bytes 6148
  184.9 51.8 %all-to-all-start.2 = ((bf16[8,64,2048]{2,1,0:T(8,128)(2,1)}), bf16[8,64,2048]{2,1,0:T(8,128)(2,1)}, u32[]{:S(2)}, u32[]{:S(2)}) async-start(bf16[8,64,2048]{2,1,0:T(8,128)(2,1)} %bitcast.101), calls=%async_computation.2 | async-start | bytes 4194304 | tf_op jit(solution)/shard_map/all_to_all | solution.py:157
  249.2 9.0 %copy-start.3 = (bf16[256,2048]{1,0:T(8,128)(2,1)S(1)}, bf16[256,2048]{1,0:T(8,128)(2,1)}, u32[]{:S(2)}) copy-start(bf16[256,2048]{1,0:T(8,128)(2,1)} %copy-done.2) | copy-start | bytes 3145732
Sparse Core Ops, SparseCore 0:
  8.9 60.9 all-gather.1
where the time goes:
time: 267 us; the launch traced here: 266 us
  waiting for transfers between devices  59.3 us (22%)
  blocking collectives  56.4 us (21%)
  local copies, waits for them, and re-layouts  43.4 us (16%)
  matrix products  33.4 us (13%)
  other arithmetic  33.2 us (12%)
  starting transfers between devices  26.8 us (10%)
  between operations  13.8 us (5%)
    all_to_all x1, blocking collectives, per_device(): lax.all_to_all(outgoing, 'sp', split_axis=0, concat_axis=0, tiled=True)  56.4 us
    all_to_all x1, waiting for transfers between devices, per_device(): lax.all_to_all(produced.reshape(incoming.shape), 'sp', split_axis=0, conc...  46.9 us
    ppermute x3, starting transfers between devices, extended(): lax.ppermute(lax.slice_in_dim(block, block.shape[dim] - width, None, axis...  14.4 us
    all_to_all x1, waiting for transfers between devices, per_device(): lax.all_to_all(attended, 'tp', split_axis=0, concat_axis=1, tiled=True)  11.6 us
    reduce_sum x2, other arithmetic, attend(): jnp.sum(exponent, axis=3, keepdims=True) + jnp.exp(sink_col - row_top)  9.89 us
    dot_general x2, matrix products, attend(): jnp.einsum('qgrd,kgd->grqk', query_heads, key_heads, preferred_element_ty...  9.67 us
    dot_general x2, matrix products, attend(): jnp.einsum('grqk,kgd->qgrd', attn_weight, value_heads, preferred_element_...  9.31 us
    reduce_sum x1, other arithmetic, per_device(): jnp.sum(route_weights[:, :, None] * route_out.astype(jnp.float32), axis=1)  8.96 us
  transfers between devices with their start and end apart: 9, of which 2 were waited for; matrix products, arithmetic and copies ran while one was open for 24% of the time, Pallas kernels for 0%

commit v1 on v0

--- a/solution.py
+++ b/solution.py
@@ -1,10 +1,16 @@
+import functools
+
 import jax
 import jax.numpy as jnp
 from jax import lax
+from jax.experimental import pallas as pl
+from jax.experimental.pallas import tpu as pltpu
 from jax.sharding import PartitionSpec as P
 
 HD = 64
 WINDOW = 128
+GROUPS = 4
+CHUNKS = 4
 
 
 neg_fill = -1e30
@@ -71,6 +77,236 @@
         extended(value_rows, (("sp", 0),), WINDOW),
         extended(doc_float, (("sp", 0),), WINDOW),
     )
+
+
+def moe_kernel(
+    groups, chunks,
+    stream_ref, gain_ref, routes_ref, rw_ref, gate_hbm, up_hbm, down_hbm,
+    out_ref,
+    send, own, peer, pout, pin, comb, ret, wsend, wown, wpeer,
+    gv, uv, dv, acc_g, acc_u,
+    zs, zr, xs, xr, zws, zwr, xws, xwr, bzs, bzr, bxs, bxr, wsem,
+):
+    me = lax.axis_index("sp")
+    gz = me // 2
+    side = me % 2
+    mate = gz * 2 + 1 - side
+    rows, width = stream_ref.shape
+    cap = rows // groups
+    cw = width // chunks
+    half = groups // 2
+    offsets = [half] + [d for d in range(groups - 1, 0, -1) if d != half]
+
+    def remote(src, dst, ss, rs, target):
+        return pltpu.make_async_remote_copy(
+            src_ref=src, dst_ref=dst, send_sem=ss, recv_sem=rs,
+            device_id={"sp": target}, device_id_type=pl.DeviceIdType.MESH,
+        )
+
+    barrier = pltpu.get_barrier_semaphore()
+    for d in offsets:
+        pl.semaphore_signal(
+            barrier, inc=1, device_id={"sp": ((gz + d) % groups) * 2 + side},
+            device_id_type=pl.DeviceIdType.MESH,
+        )
+    pl.semaphore_signal(
+        barrier, inc=1, device_id={"sp": mate}, device_id_type=pl.DeviceIdType.MESH
+    )
+    loads = [
+        pltpu.make_async_copy(s.at[0], t, wsem.at[i])
+        for i, (s, t) in enumerate(((gate_hbm, gv), (up_hbm, uv), (down_hbm, dv)))
+    ]
+    for load in loads:
+        load.start()
+
+    stream_f = stream_ref[...].astype(jnp.float32)
+    scale = lax.rsqrt(jnp.mean(stream_f * stream_f, axis=1, keepdims=True) + eps_norm)
+    normed = (stream_f * scale * gain_ref[...]).astype(jnp.bfloat16)
+
+    first = routes_ref[:, 0:1]
+    group_of = first // 2
+    lanes = lax.broadcasted_iota(jnp.int32, (rows, 128), 1)
+    one_hot = jnp.where(group_of == lanes, 1.0, 0.0)
+    ri = lax.broadcasted_iota(jnp.int32, (rows, rows), 0)
+    ci = lax.broadcasted_iota(jnp.int32, (rows, rows), 1)
+    below = jnp.where(ci < ri, 1.0, 0.0).astype(jnp.bfloat16)
+    ranks = jnp.dot(below, one_hot.astype(jnp.bfloat16), preferred_element_type=jnp.float32)
+    slot = group_of.astype(jnp.float32) * cap + jnp.sum(ranks * one_hot, axis=1, keepdims=True)
+    spread = jnp.where(slot == ci.astype(jnp.float32), 1.0, 0.0)
+    spread_b = spread.astype(jnp.bfloat16)
+    slot_lane = jnp.sum(jnp.where(ri == ci, slot, 0.0), axis=0, keepdims=True)
+    pick = jnp.where(ri.astype(jnp.float32) == slot_lane, 1.0, 0.0).astype(jnp.bfloat16)
+    for parity in range(2):
+        w_col = jnp.where(first % 2 == parity, rw_ref[:, 0:1], rw_ref[:, 1:2])
+        w_row = jnp.sum(spread * w_col, axis=0, keepdims=True)
+        wsend[parity] = jnp.broadcast_to(w_row, (8, rows))
+
+    pl.semaphore_wait(barrier, groups)
+
+    pending = []
+    for d in offsets:
+        copy = remote(wsend, wown.at[gz], zws.at[d], zwr.at[gz], ((gz + d) % groups) * 2 + side)
+        copy.start()
+        pending.append(copy)
+    copy = remote(wsend, wpeer.at[gz], xws.at[gz], xwr.at[gz], mate)
+    copy.start()
+    pending.append(copy)
+
+    for j in range(chunks):
+        piece = jnp.dot(pick, normed[:, j * cw:(j + 1) * cw], preferred_element_type=jnp.float32)
+        send[j] = piece.astype(jnp.bfloat16).reshape(groups, cap, cw)
+        for d in offsets:
+            target = (gz + d) % groups
+            copy = remote(
+                send.at[j, target], own.at[j, gz], zs.at[j, d], zr.at[j, gz], target * 2 + side
+            )
+            copy.start()
+            pending.append(copy)
+        copy = remote(send.at[j, gz], peer.at[j, gz], xs.at[j, gz], xr.at[j, gz], mate)
+        copy.start()
+        pending.append(copy)
+        own[j, pl.ds(gz, 1)] = send[j, pl.ds(gz, 1)]
+    wown[pl.ds(gz, 1)] = wsend[...][None]
+
+    for d in offsets:
+        source = (gz + groups - d) % groups
+        remote(wsend, wown.at[source], zws.at[d], zwr.at[source], mate).wait_recv()
+        copy = remote(wown.at[source], wpeer.at[source], xws.at[source], xwr.at[source], mate)
+        copy.start()
+        pending.append(copy)
+
+    loads[0].wait()
+    loads[1].wait()
+
+    def accumulate(buf, j, base):
+        block = buf[j].reshape(rows, cw)
+        part_g = jnp.dot(block, gv[j * cw:(j + 1) * cw, :], preferred_element_type=jnp.float32)
+        part_u = jnp.dot(block, uv[j * cw:(j + 1) * cw, :], preferred_element_type=jnp.float32)
+        if j == 0:
+            acc_g[base:base + rows, :] = part_g
+            acc_u[base:base + rows, :] = part_u
+        else:
+            acc_g[base:base + rows, :] += part_g
+            acc_u[base:base + rows, :] += part_u
+
+    def peer_step(j):
+        for s in range(groups):
+            remote(send.at[j, s], peer.at[j, s], xs.at[j, s], xr.at[j, s], mate).wait_recv()
+        accumulate(peer, j, rows)
+
+    for j in range(chunks):
+        for d in offsets:
+            source = (gz + groups - d) % groups
+            remote(
+                send.at[j, source], own.at[j, source], zs.at[j, d], zr.at[j, source], mate
+            ).wait_recv()
+            copy = remote(
+                own.at[j, source], peer.at[j, source], xs.at[j, source], xr.at[j, source], mate
+            )
+            copy.start()
+            pending.append(copy)
+        accumulate(own, j, 0)
+        if j:
+            peer_step(j - 1)
+    peer_step(chunks - 1)
+    for s in range(groups):
+        remote(wsend, wpeer.at[s], xws.at[s], xwr.at[s], mate).wait_recv()
+
+    def hidden_of(base):
+        g = acc_g[base:base + rows, :]
+        return (g / (1.0 + jnp.exp(-g)) * acc_u[base:base + rows, :]).astype(jnp.bfloat16)
+
+    sub = lax.broadcasted_iota(jnp.int32, (cap, rows), 0)
+    lane = lax.broadcasted_iota(jnp.int32, (cap, rows), 1)
+    chosen = lane == sub + gz * cap
+
+    def weights_of(buf):
+        cols = []
+        for s in range(groups):
+            row = jnp.where(side == 0, buf[s, 0, 0:1, :], buf[s, 1, 0:1, :])
+            cols.append(jnp.sum(jnp.where(chosen, row, 0.0), axis=1, keepdims=True))
+        return jnp.concatenate(cols, axis=0)
+
+    w_peer = weights_of(wpeer)
+    hid_peer = hidden_of(rows)
+    loads[2].wait()
+    for j in range(chunks):
+        part = jnp.dot(hid_peer, dv[:, j * cw:(j + 1) * cw], preferred_element_type=jnp.float32)
+        pout[j] = (part * w_peer).astype(jnp.bfloat16)
+        copy = remote(pout.at[j], pin.at[j], bxs.at[j], bxr.at[j], mate)
+        copy.start()
+        pending.append(copy)
+    w_own = weights_of(wown)
+    hid_own = hidden_of(0)
+    for j in range(chunks):
+        part = jnp.dot(hid_own, dv[:, j * cw:(j + 1) * cw], preferred_element_type=jnp.float32)
+        remote(pout.at[j], pin.at[j], bxs.at[j], bxr.at[j], mate).wait_recv()
+        total = part * w_own + pin[j].astype(jnp.float32)
+        comb[j] = total.astype(jnp.bfloat16).reshape(groups, cap, cw)
+        for d in offsets:
+            target = (gz + d) % groups
+            copy = remote(
+                comb.at[j, target], ret.at[j, gz], bzs.at[j, d], bzr.at[j, gz], target * 2 + side
+            )
+            copy.start()
+            pending.append(copy)
+        ret[j, pl.ds(gz, 1)] = comb[j, pl.ds(gz, 1)]
+    for j in range(chunks):
+        for d in offsets:
+            source = (gz + groups - d) % groups
+            remote(
+                comb.at[j, source], ret.at[j, source], bzs.at[j, d], bzr.at[j, source], mate
+            ).wait_recv()
+        back = jnp.dot(spread_b, ret[j].reshape(rows, cw), preferred_element_type=jnp.float32)
+        cols = slice(j * cw, (j + 1) * cw)
+        out_ref[:, cols] = (stream_ref[:, cols].astype(jnp.float32) + back).astype(jnp.bfloat16)
+    for copy in pending:
+        copy.wait_send()
+
+
+def pair_routed(routes, gate_weight):
+    count = lax.axis_size("sp")
+    experts = count * gate_weight.shape[0]
+    return (
+        gate_weight.shape[0] == 1
+        and routes.shape[1] == 2
+        and experts == 2 * GROUPS
+    )
+
+
+def mixture(stream, norm_gain, routes, route_weights, gate_weight, up_weight, down_weight):
+    rows, width = stream.shape
+    ff = gate_weight.shape[2]
+    groups = lax.axis_size("sp") // 2
+    cap, cw = rows // groups, width // CHUNKS
+    bf, f32 = jnp.bfloat16, jnp.float32
+    quad = pltpu.VMEM((CHUNKS, groups, cap, cw), bf)
+    flat = pltpu.VMEM((CHUNKS, rows, cw), bf)
+    dma = pltpu.SemaphoreType.DMA
+    vm = pl.BlockSpec(memory_space=pltpu.VMEM)
+    hbm = pl.BlockSpec(memory_space=pl.ANY)
+    return pl.pallas_call(
+        functools.partial(moe_kernel, groups, CHUNKS),
+        out_shape=jax.ShapeDtypeStruct((rows, width), bf),
+        in_specs=[vm] * 4 + [hbm] * 3,
+        out_specs=vm,
+        scratch_shapes=[
+            quad, quad, quad, flat, flat, quad, quad,
+            pltpu.VMEM((2, 8, rows), f32),
+            pltpu.VMEM((groups, 2, 8, rows), f32),
+            pltpu.VMEM((groups, 2, 8, rows), f32),
+            pltpu.VMEM((width, ff), bf), pltpu.VMEM((width, ff), bf), pltpu.VMEM((ff, width), bf),
+            pltpu.VMEM((2 * rows, ff), f32), pltpu.VMEM((2 * rows, ff), f32),
+            dma((CHUNKS, groups)), dma((CHUNKS, groups)), dma((CHUNKS, groups)), dma((CHUNKS, groups)),
+            dma((groups,)), dma((groups,)), dma((groups,)), dma((groups,)),
+            dma((CHUNKS, groups)), dma((CHUNKS, groups)), dma((CHUNKS,)), dma((CHUNKS,)),
+            dma((3,)),
+        ],
+        compiler_params=pltpu.CompilerParams(
+            collective_id=3, has_side_effects=True, vmem_limit_bytes=48 * 1024 * 1024
+        ),
+        name="mixture",
+    )(stream, norm_gain[None, :], routes, route_weights, gate_weight, up_weight, down_weight)
 
 
 def per_device(
@@ -125,6 +361,10 @@
         )
         running = running + partial_value.astype(jnp.bfloat16).astype(jnp.float32)
     stream = (residual.astype(jnp.float32) + running).astype(jnp.bfloat16)
+    if pair_routed(routes, gate_weight):
+        return mixture(
+            stream, norm_gain, routes, route_weights, gate_weight, up_weight, down_weight
+        )
     stream_f = stream.astype(jnp.float32)
     scale = lax.rsqrt(jnp.mean(stream_f * stream_f, axis=1, keepdims=True) + eps_norm)
     normed = (stream_f * scale * norm_gain[None, :]).astype(jnp.bfloat16)

time: 267 us -> 169 us (0.63)
  Pallas kernels: 0 us -> 67.7 us
  blocking collectives: 56.4 us -> 0 us
  waiting for transfers between devices: 59.3 us -> 17.1 us
  local copies, waits for them, and re-layouts: 43.4 us -> 6.83 us
  other arithmetic: 33.2 us -> 14.2 us
  matrix products: 33.4 us -> 26.9 us
  starting transfers between devices: 26.8 us -> 22 us
    pallas_call x0 -> x1, Pallas kernels: none -> 67.7 us  [mixture(): pl.pallas_call(functools.partial(moe_kernel, groups, CHUNKS), out_shape=j...]
    all_to_all x1 -> x0, blocking collectives: 56.4 us -> none  [per_device(): lax.all_to_all(outgoing, 'sp', split_axis=0, concat_axis=0, tiled=True)]
    all_to_all x1 -> x0, waiting for transfers between devices: 46.9 us -> none  [per_device(): lax.all_to_all(produced.reshape(incoming.shape), 'sp', split_axis=0, conc...]
    gather x2 -> x0, local copies, waits for them, and re-layouts: 10.4 us -> none  [the longest x1 7.1 us: per_device(): returned.reshape(-1, width)[slot_index]]
    reduce_sum x2 -> x0, other arithmetic: 9.05 us -> none  [the longest x1 8.96 us: per_device(): jnp.sum(route_weights[:, :, None] * route_out.astype(jnp.float32), axis=1)]
    dot_general x2 -> x0, matrix products: 7.22 us -> none  [the longest x1 5.98 us: per_device(): jnp.dot(hidden, down_weight[0], preferred_element_type=jnp.float32)]
    convert_element_type x1 -> x0, local copies, waits for them, and re-layouts: 5.43 us -> none  [per_device(): route_out.astype(jnp.float32)]
    unnamed x52 -> x17, local copies, waits for them, and re-layouts: 6 us -> 1.28 us
  transfers between devices with their start and end apart: 9 -> 8, of which waited for: 2 -> 2; matrix products, arithmetic and copies ran while one was open for 24% -> 24% of each run, Pallas kernels for 0% -> 0%
where the time goes in v1:
time: 169 us; the launch traced here: 168 us
  Pallas kernels  67.7 us (40%)
  matrix products  26.9 us (16%)
  starting transfers between devices  22 us (13%)
  waiting for transfers between devices  17.1 us (10%)
  other arithmetic  14.2 us (8%)
  between operations  13.8 us (8%)
  local copies, waits for them, and re-layouts  6.83 us (4%)
    pallas_call x1, Pallas kernels, mixture(): pl.pallas_call(functools.partial(moe_kernel, groups, CHUNKS), out_shape=j...  67.7 us
    ppermute x3, starting transfers between devices, extended(): lax.ppermute(lax.slice_in_dim(block, block.shape[dim] - width, None, axis...  14.4 us
    all_to_all x1, waiting for transfers between devices, per_device(): lax.all_to_all(attended, 'tp', split_axis=0, concat_axis=1, tiled=True)  13.9 us
    dot_general x2, matrix products, attend(): jnp.einsum('grqk,kgd->qgrd', attn_weight, value_heads, preferred_element_...  11.1 us
    reduce_sum x2, other arithmetic, attend(): jnp.sum(exponent, axis=3, keepdims=True) + jnp.exp(sink_col - row_top)  9.61 us
    dot_general x2, matrix products, attend(): jnp.einsum('qgrd,kgd->grqk', query_heads, key_heads, preferred_element_ty...  8.68 us
    dot_general x4, matrix products, per_device(): jnp.dot(columns, weight_piece[shard_index * shard_rows:(shard_index + 1)...  7.12 us
    ppermute x3, starting transfers between devices, extended(): lax.ppermute(lax.slice_in_dim(block, 0, width, axis=dim), axis, backward)  3.88 us
  transfers between devices with their start and end apart: 8, of which 2 were waited for; matrix products, arithmetic and copies ran while one was open for 24% of the time, Pallas kernels for 0%

profile of v1, /device:TPU:0, one launch (start us, length us, event | category | flops | bytes accessed | tf_op | source)
XLA Modules:
  0.0 168.5 jit_solution(9837957539400235503)
XLA Ops:
  6.5 0.7 all-gather.2.cloned.1.call-update
  7.3 0.7 convert_element_type.52
  8.0 4.9 %collective-permute-start.1 = (bf16[128]{0:T(256)(128)(2,1)S(1)}, bf16[128]{0:T(256)(128)(2,1)S(1)}, u32[]{:S(2)}, u32[]{:S(2)}) collective-permute-start(bf16[128]{0:T(256)(128)(2,1)S(1)} %get-tuple-element.17), channel_id=1, source_target_pairs={{0,4},{4,8},{8,12},{12,16},{16,20},{20,24},{24,28},{1,5},{5,9},{9,... | collective-permute-start | bytes 776 | tf_op jit(solution)/shard_map/ppermute | solution.py:25
  12.8 1.3 collective-permute-start.4
  14.1 0.8 fusion.36
  14.9 4.5 %collective-permute-start.2 = (bf16[128,128]{1,0:T(8,128)(2,1)S(1)}, bf16[128,128]{1,0:T(8,128)(2,1)S(1)}, u32[]{:S(2)}, u32[]{:S(2)}) collective-permute-start(bf16[128,128]{1,0:T(8,128)(2,1)S(1)} %get-tuple-element.9), channel_id=1, source_target_pairs={{0,4},{4,8},{8,12},{12,16},{16,20},{20,24},{24,28},{1,5},{5,9},{9,... | collective-permute-start | bytes 98312 | tf_op jit(solution)/shard_map/ppermute | solution.py:25
  19.5 1.3 collective-permute-start.5
  20.8 0.8 fusion.37
  21.5 5.0 %collective-permute-start = (bf16[128,128]{1,0:T(8,128)(2,1)S(1)}, bf16[128,128]{1,0:T(8,128)(2,1)S(1)}, u32[]{:S(2)}, u32[]{:S(2)}) collective-permute-start(bf16[128,128]{1,0:T(8,128)(2,1)S(1)} %get-tuple-element.13), channel_id=1, source_target_pairs={{0,4},{4,8},{8,12},{12,16},{16,20},{20,24},{24,28},{1,5},{5,9},{9,... | collective-permute-start | bytes 98312 | tf_op jit(solution)/shard_map/ppermute | solution.py:25
  26.7 1.3 fusion.35
  27.9 0.2 copy.36
  28.1 0.7 max.32
  28.9 0.2 copy.40
  29.1 1.3 collective-permute-start.3
  30.4 1.5 fusion.21
  32.0 1.0 pad_maximum_fusion.3
  33.0 0.1 copy.35
  33.2 0.1 copy.39
  33.3 2.5 %collective-permute-done.3 = bf16[128,128]{1,0:T(8,128)(2,1)S(1)} collective-permute-done((bf16[128,128]{1,0:T(8,128)(2,1)S(1)}, bf16[128,128]{1,0:T(8,128)(2,1)S(1)}, u32[]{:S(2)}, u32[]{:S(2)}) %collective-permute-start.3) | collective-permute-done | bytes 32800 | tf_op jit(solution)/shard_map/ppermute | solution.py:28
  35.8 0.1 copy.34
  36.0 2.1 %fusion = (f32[2,4,512]{2,1,0:T(4,128)S(1)}, f32[2,768,512,4]{2,1,3,0:T(8,128)S(1)}) fusion(pred[512,768]{0,1:T(8,128)(4,1)S(1)} %get-tuple-element.28, bf16[768,2,64,1]{0,2,3,1:T(8,128)(2,1)S(1)} %bitcast.73, bf16[512,2,4,64]{0,3,2,1:T(8,128)(2,1)S(1)} %bitcast.71), kind=kOutput, calls=%fused_computation.6 | convolution fusion | flops 412086272 | bytes 13713408 | tf_op jit(solution)/shard_map/qgrd,kgd->grqk/dot_general | solution.py:51
  38.1 0.1 broadcast_maximum_fusion.1
  38.2 6.6 %fusion.1 = (f32[2,4,512]{2,1,0:T(4,128)S(1)}, f32[2,768,512,4]{2,1,3,0:T(8,128)}) fusion(pred[512,768]{0,1:T(8,128)(4,1)S(1)} %get-tuple-element.27, bf16[768,2,64,1]{0,2,3,1:T(8,128)(2,1)S(1)} %bitcast.72, bf16[512,2,4,64]{0,3,2,1:T(8,128)(2,1)S(1)} %bitcast.70), kind=kOutput, calls=%fused_computation.7 | convolution fusion | flops 412086272 | bytes 13713408 | tf_op jit(solution)/shard_map/qgrd,kgd->grqk/dot_general | solution.py:51
  44.7 3.1 %fusion.2 = f32[2,4,512]{2,1,0:T(4,128)S(1)} fusion(f32[2,768,512,4]{2,1,3,0:T(8,128)S(1)} %get-tuple-element.24, f32[2,4,512]{2,1,0:T(4,128)S(1)} %broadcast_maximum_fusion.1, pred[512,768]{0,1:T(8,128)(4,1)S(1)} %get-tuple-element.28), kind=kLoop, calls=%fused_computation.8 | loop fusion | flops 15724544 | bytes 13008896 | tf_op jit(solution)/shard_map/reduce_sum | solution.py:66
  47.8 0.1 exponential_add_fusion.1
  47.9 3.9 %fusion.24 = bf16[2,64,4,512]{3,1,2,0:T(8,128)(2,1)S(1)} fusion(bf16[768,2,64,1]{0,2,3,1:T(8,128)(2,1)S(1)} %bitcast.76, f32[2,768,512,4]{2,1,3,0:T(8,128)S(1)} %get-tuple-element.24, f32[2,4,512]{2,1,0:T(4,128)S(1)} %get-tuple-element.21, f32[2,4,512]{2,1,0:T(4,128)S(1)} %broadcast_maximum_fusion.1, pred[512,768]{0,1:T(8,128)(4,1)S(1)} %get-tuple-element.28), kind=kOutput, calls=%fused_computation.36 | convolution fusion | flops 421789696 | bytes 13729792 | tf_op jit(solution)/shard_map/grqk,kgd->qgrd/dot_general | solution.py:68
  51.9 0.2 copy.42
  52.1 0.1 copy.38
  52.2 6.5 %fusion.3 = f32[2,4,512]{2,1,0:T(4,128)S(1)} fusion(f32[2,768,512,4]{2,1,3,0:T(8,128)} %get-tuple-element.26, f32[2,4,512]{2,1,0:T(4,128)S(1)} %get-tuple-element.22, pred[512,768]{0,1:T(8,128)(4,1)S(1)} %get-tuple-element.27), kind=kLoop, calls=%fused_computation.9 | loop fusion | flops 15724544 | bytes 13008896 | tf_op jit(solution)/shard_map/reduce_sum | solution.py:66
  58.8 0.1 exponential_add_fusion
  58.9 0.0 copy-start.5
  58.9 0.0 copy-start.6
  58.9 7.2 %fusion.23 = bf16[2,64,4,512]{3,1,2,0:T(8,128)(2,1)S(1)} fusion(bf16[768,2,64,1]{0,2,3,1:T(8,128)(2,1)S(1)} %bitcast.77, f32[2,768,512,4]{2,1,3,0:T(8,128)} %get-tuple-element.26, f32[2,4,512]{2,1,0:T(4,128)S(1)} %exponential_add_fusion, f32[2,4,512]{2,1,0:T(4,128)S(1)} %get-tuple-element.22, pred[512,768]{0,1:T(8,128)(4,1)S(1)} %get-tuple-element.27), kind=kOutput, calls=%fused_computation.35 | convolution fusion | flops 421789696 | bytes 13729792 | tf_op jit(solution)/shard_map/grqk,kgd->qgrd/dot_general | solution.py:68
  66.1 0.2 copy.43
  66.3 1.0 pad_maximum_fusion
  67.3 3.7 %all-to-all-start = ((bf16[4,256,512]{2,1,0:T(8,128)(2,1)}), bf16[4,256,512]{2,1,0:T(8,128)(2,1)S(1)}, u32[]{:S(2)}, u32[]{:S(2)}) async-start(bf16[4,256,512]{2,1,0:T(8,128)(2,1)} %bitcast.20), calls=%async_computation | async-start | bytes 2097152 | tf_op jit(solution)/shard_map/all_to_all | solution.py:350
  71.0 0.0 copy-start.3
  71.0 0.1 copy.45.routes_ref
  71.2 0.1 copy.46.rw_ref
  71.3 13.9 %all-to-all-done = bf16[4,256,512]{2,1,0:T(8,128)(2,1)S(1)} async-done(((bf16[4,256,512]{2,1,0:T(8,128)(2,1)}), bf16[4,256,512]{2,1,0:T(8,128)(2,1)S(1)}, u32[]{:S(2)}, u32[]{:S(2)}) %all-to-all-start) | async-done | bytes 1048608 | tf_op jit(solution)/shard_map/all_to_all | solution.py:350
  85.2 0.5 copy.44
  85.8 0.0 all-gather.2.cloned.1.call-done
  85.8 2.5 %fusion.12 = f32[256,2048]{1,0:T(8,128)S(1)} fusion(bf16[2048,2048]{1,0:T(8,128)(2,1)} %all-gather.2.cloned.1.call-done, bf16[256,2048]{0,1:T(8,128)(2,1)S(1)} %bitcast.66), kind=kOutput, calls=%fused_computation.22 | convolution fusion | flops 537919488 | bytes 4456448 | tf_op jit(solution)/shard_map/dot_general | solution.py:357
  88.3 2.9 %fusion.13 = f32[256,2048]{1,0:T(8,128)S(1)} fusion(bf16[2048,2048]{1,0:T(8,128)(2,1)} %all-gather.2.cloned.1.call-done, bf16[256,2048]{0,1:T(8,128)(2,1)S(1)} %bitcast.67), kind=kOutput, calls=%fused_computation.23 | convolution fusion | flops 537919488 | bytes 4456448 | tf_op jit(solution)/shard_map/dot_general | solution.py:357
  91.2 0.7 fusion.14
  91.9 1.1 fusion.11.stream_ref
  93.0 67.7 %mixture.1 = bf16[256,2048]{1,0:T(8,128)(2,1)S(1)} custom-call(bf16[256,2048]{1,0:T(8,128)(2,1)S(1)} %fusion.11.stream_ref, f32[1,2048]{1,0:T(1,128)S(1)} %bitcast.64, s32[256,2]{1,0:T(8,128)S(1)} %copy.45.routes_ref, f32[256,2]{1,0:T(8,128)S(1)} %copy.46.rw_ref, bf16[1,2048,512]{2,1,0:T(8,128)(2,1)S(1)} %copy-done, bf16[1,2048,512]{2,1,0:T(8,128)(2,1)} %up_hbm.1, ...), custom_call_target="tpu_custom_call" | custom-call | tf_op jit(solution)/shard_map/mixture/pallas_call | solution.py:288
  160.7 1.0 copy.54
  (27 shorter events, 0.1 us)
Async XLA Ops:
  6.5 29.3 %copy-start.4 = (bf16[1024,128]{1,0:T(8,128)(2,1)S(1)}, bf16[1024,128]{1,0:T(8,128)(2,1)}, u32[]{:S(2)}) copy-start(bf16[1024,128]{1,0:T(8,128)(2,1)} %param.15) | copy-start | bytes 786436
  6.5 79.2 %all-gather.2.cloned.1.call-start = ((), (), s32[]{:S(2)}) async-start(), calls=%async_computation.1 | async-start | bytes 10485760 | tf_op jit(solution)/shard_map/all_gather | solution.py:354
  8.0 21.1 %collective-permute-start.1 = (bf16[128]{0:T(256)(128)(2,1)S(1)}, bf16[128]{0:T(256)(128)(2,1)S(1)}, u32[]{:S(2)}, u32[]{:S(2)}) collective-permute-start(bf16[128]{0:T(256)(128)(2,1)S(1)} %get-tuple-element.17), channel_id=1, source_target_pairs={{0,4},{4,8},{8,12},{12,16},{16,20},{20,24},{24,28},{1,5},{5,9},{9,... | collective-permute-start | bytes 776 | tf_op jit(solution)/shard_map/ppermute | solution.py:25
  12.8 17.6 %collective-permute-start.4 = (bf16[128]{0:T(256)(128)(2,1)S(1)}, bf16[128]{0:T(256)(128)(2,1)S(1)}, u32[]{:S(2)}, u32[]{:S(2)}) collective-permute-start(bf16[128]{0:T(256)(128)(2,1)S(1)} %get-tuple-element.18), channel_id=1, source_target_pairs={{4,0},{8,4},{12,8},{16,12},{20,16},{24,20},{28,24},{5,1},{9,5},{13... | collective-permute-start | bytes 776 | tf_op jit(solution)/shard_map/ppermute | solution.py:28
  14.9 17.1 %collective-permute-start.2 = (bf16[128,128]{1,0:T(8,128)(2,1)S(1)}, bf16[128,128]{1,0:T(8,128)(2,1)S(1)}, u32[]{:S(2)}, u32[]{:S(2)}) collective-permute-start(bf16[128,128]{1,0:T(8,128)(2,1)S(1)} %get-tuple-element.9), channel_id=1, source_target_pairs={{0,4},{4,8},{8,12},{12,16},{16,20},{20,24},{24,28},{1,5},{5,9},{9,... | collective-permute-start | bytes 98312 | tf_op jit(solution)/shard_map/ppermute | solution.py:25
  19.5 12.5 %collective-permute-start.5 = (bf16[128,128]{1,0:T(8,128)(2,1)S(1)}, bf16[128,128]{1,0:T(8,128)(2,1)S(1)}, u32[]{:S(2)}, u32[]{:S(2)}) collective-permute-start(bf16[128,128]{1,0:T(8,128)(2,1)S(1)} %get-tuple-element.10), channel_id=1, source_target_pairs={{4,0},{8,4},{12,8},{16,12},{20,16},{24,20},{28,24},{5,1},{9,5},{13... | collective-permute-start | bytes 98312 | tf_op jit(solution)/shard_map/ppermute | solution.py:28
  21.5 11.8 %collective-permute-start = (bf16[128,128]{1,0:T(8,128)(2,1)S(1)}, bf16[128,128]{1,0:T(8,128)(2,1)S(1)}, u32[]{:S(2)}, u32[]{:S(2)}) collective-permute-start(bf16[128,128]{1,0:T(8,128)(2,1)S(1)} %get-tuple-element.13), channel_id=1, source_target_pairs={{0,4},{4,8},{8,12},{12,16},{16,20},{20,24},{24,28},{1,5},{5,9},{9,... | collective-permute-start | bytes 98312 | tf_op jit(solution)/shard_map/ppermute | solution.py:25
  29.1 6.7 %collective-permute-start.3 = (bf16[128,128]{1,0:T(8,128)(2,1)S(1)}, bf16[128,128]{1,0:T(8,128)(2,1)S(1)}, u32[]{:S(2)}, u32[]{:S(2)}) collective-permute-start(bf16[128,128]{1,0:T(8,128)(2,1)S(1)} %get-tuple-element.14), channel_id=1, source_target_pairs={{4,0},{8,4},{12,8},{16,12},{20,16},{24,20},{28,24},{5,1},{9,5},{13... | collective-permute-start | bytes 98312 | tf_op jit(solution)/shard_map/ppermute | solution.py:28
  58.9 12.2 %copy-start.5 = (s32[256,2]{0,1:T(2,128)S(1)}, s32[256,2]{0,1:T(2,128)}, u32[]{:S(2)}) copy-start(s32[256,2]{0,1:T(2,128)} %param.24) | copy-start | bytes 6148
  58.9 12.3 %copy-start.6 = (f32[256,2]{0,1:T(2,128)S(1)}, f32[256,2]{0,1:T(2,128)}, u32[]{:S(2)}) copy-start(f32[256,2]{0,1:T(2,128)} %param.25) | copy-start | bytes 6148
  67.3 17.9 %all-to-all-start = ((bf16[4,256,512]{2,1,0:T(8,128)(2,1)}), bf16[4,256,512]{2,1,0:T(8,128)(2,1)S(1)}, u32[]{:S(2)}, u32[]{:S(2)}) async-start(bf16[4,256,512]{2,1,0:T(8,128)(2,1)} %bitcast.20), calls=%async_computation | async-start | bytes 2097152 | tf_op jit(solution)/shard_map/all_to_all | solution.py:350
  71.0 20.9 %copy-start.3 = (bf16[256,2048]{1,0:T(8,128)(2,1)S(1)}, bf16[256,2048]{1,0:T(8,128)(2,1)}, u32[]{:S(2)}) copy-start(bf16[256,2048]{1,0:T(8,128)(2,1)} %param.18) | copy-start | bytes 3145732
  85.8 5.3 %copy-start.2 = (bf16[2048,2048]{1,0:T(8,128)(2,1)S(1)}, bf16[2048,2048]{1,0:T(8,128)(2,1)}, u32[]{:S(2)}) copy-start(bf16[2048,2048]{1,0:T(8,128)(2,1)} %all-gather.2.cloned.1.call-done) | copy-start | bytes 25165828
  91.1 1.8 %copy-start = (bf16[1,2048,512]{2,1,0:T(8,128)(2,1)S(1)}, bf16[1,2048,512]{2,1,0:T(8,128)(2,1)}, u32[]{:S(2)}) copy-start(bf16[1,2048,512]{2,1,0:T(8,128)(2,1)} %gate_hbm.1) | copy-start | bytes 6291460
  91.1 1.8 %copy-start.1 = (f32[2048]{0:T(1024)S(1)}, f32[2048]{0:T(1024)}, u32[]{:S(2)}) copy-start(f32[2048]{0:T(1024)} %param.20) | copy-start | bytes 24580
Sparse Core Ops, SparseCore 0:
  8.9 60.9 all-gather.1

commit v2 on v1

--- a/solution.py
+++ b/solution.py
@@ -264,6 +264,185 @@
         copy.wait_send()
 
 
+def front_kernel(
+    chunks,
+    sink_ref, q_ref, k_ref, v_ref, doc_ref, res_ref, w_ref,
+    out_ref,
+    kx, vx, dl, dr, dx, att, am_far, am_near, w_mate, acc, ysend, yrecv,
+    hs, hr, ms, mr, ys, yr,
+):
+    sp = lax.axis_index("sp")
+    tp = lax.axis_index("tp")
+    sp_count = lax.axis_size("sp")
+    mate = tp + 1 - 2 * (tp % 2)
+    across = (tp + 2) % 4
+    mate_across = (mate + 2) % 4
+    after = (sp + 1) % sp_count
+    before = (sp + sp_count - 1) % sp_count
+    blocks = q_ref.shape[0] // WINDOW
+    home_blocks = blocks // 4
+    half = blocks // 2
+    kv_heads = k_ref.shape[1] // HD
+    ratio = q_ref.shape[1] // k_ref.shape[1]
+    width = out_ref.shape[1]
+    cw = width // chunks
+    f32, bf = jnp.float32, jnp.bfloat16
+    mesh_id = pl.DeviceIdType.MESH
+
+    def remote(src, dst, ss, rs, where):
+        return pltpu.make_async_remote_copy(
+            src_ref=src, dst_ref=dst, send_sem=ss, recv_sem=rs,
+            device_id=where, device_id_type=mesh_id,
+        )
+
+    barrier = pltpu.get_barrier_semaphore()
+    for where in ({"sp": after}, {"sp": before}, {"tp": mate}, {"tp": across}):
+        pl.semaphore_signal(barrier, inc=1, device_id=where, device_id_type=mesh_id)
+    for b in range(blocks):
+        kx[b + 1] = k_ref[b * WINDOW:(b + 1) * WINDOW, :]
+        vx[b + 1] = v_ref[b * WINDOW:(b + 1) * WINDOW, :]
+        dx[b + 1] = jnp.broadcast_to(doc_ref[b:b + 1, :].astype(f32), (8, WINDOW))
+    pl.semaphore_wait(barrier, 4)
+
+    tail = pl.ds((blocks - 1) * WINDOW, WINDOW)
+    lead = pl.ds(0, WINDOW)
+    halo = [
+        remote(k_ref.at[tail], kx.at[0], hs.at[0], hr.at[0], {"sp": after}),
+        remote(v_ref.at[tail], vx.at[0], hs.at[1], hr.at[1], {"sp": after}),
+        remote(doc_ref, dl, hs.at[2], hr.at[2], {"sp": after}),
+        remote(k_ref.at[lead], kx.at[blocks + 1], hs.at[3], hr.at[3], {"sp": before}),
+        remote(v_ref.at[lead], vx.at[blocks + 1], hs.at[4], hr.at[4], {"sp": before}),
+        remote(doc_ref, dr, hs.at[5], hr.at[5], {"sp": before}),
+    ]
+    for copy in halo:
+        copy.start()
+    w_copy = remote(w_ref, w_mate, ms.at[0], mr.at[0], {"tp": mate})
+    w_copy.start()
+
+    qi = lax.broadcasted_iota(jnp.int32, (WINDOW, 3 * WINDOW), 0)
+    ki = lax.broadcasted_iota(jnp.int32, (WINDOW, 3 * WINDOW), 1)
+    band = (ki >= qi) & (ki <= qi + 2 * WINDOW)
+    eye = lax.broadcasted_iota(jnp.int32, (WINDOW, WINDOW), 0) == lax.broadcasted_iota(
+        jnp.int32, (WINDOW, WINDOW), 1
+    )
+
+    def attend_block(b):
+        own_docs = dx[b + 1][0:1]
+        key_docs = jnp.concatenate([dx[b][0:1], own_docs, dx[b + 2][0:1]], axis=1)
+        query_docs = jnp.sum(jnp.where(eye, own_docs, 0.0), axis=1, keepdims=True)
+        bias = jnp.where(band & (key_docs == query_docs), 0.0, neg_fill)
+        keys = kx[pl.ds(b, 3)].reshape(3 * WINDOW, kv_heads * HD)
+        values = vx[pl.ds(b, 3)].reshape(3 * WINDOW, kv_heads * HD)
+        home = b // home_blocks
+        to_rows = pl.ds(pl.multiple_of((b % home_blocks) * WINDOW, WINDOW), WINDOW)
+        from_rows = pl.ds(pl.multiple_of(b * WINDOW, WINDOW), WINDOW)
+        for g in range(kv_heads):
+            span = slice(g * ratio * HD, (g + 1) * ratio * HD)
+            q = q_ref[from_rows, span] * jnp.asarray(HD ** (-0.5), bf)
+            stacked = jnp.concatenate([q[:, r * HD:(r + 1) * HD] for r in range(ratio)], axis=0)
+            scores = lax.dot_general(
+                stacked, keys[:, g * HD:(g + 1) * HD], (((1,), (1,)), ((), ())),
+                preferred_element_type=f32,
+            )
+            vg = values[:, g * HD:(g + 1) * HD]
+            parts = []
+            for r in range(ratio):
+                sink = sink_ref[g * ratio + r]
+                s = scores[r * WINDOW:(r + 1) * WINDOW] + bias
+                top = jnp.maximum(jnp.max(s, axis=1, keepdims=True), sink)
+                e = jnp.exp(s - top)
+                den = jnp.sum(e, axis=1, keepdims=True) + jnp.exp(sink - top)
+                o = jnp.dot(e.astype(bf), vg, preferred_element_type=f32)
+                parts.append((o / den).astype(bf))
+            att[home, to_rows, span] = jnp.concatenate(parts, axis=1)
+
+    def far_step(i, carry):
+        @pl.when(i == half - 1)
+        def _():
+            for copy in halo:
+                copy.wait_recv()
+            left = dl[blocks - 1:blocks, :].astype(f32)
+            right = dr[0:1, :].astype(f32)
+            left = jnp.where(sp == 0, -1.0, left)
+            right = jnp.where(sp == sp_count - 1, -1.0, right)
+            dx[0] = jnp.broadcast_to(left, (8, WINDOW))
+            dx[blocks + 1] = jnp.broadcast_to(right, (8, WINDOW))
+
+        attend_block(jnp.where(tp < 2, half + i, half - 1 - i))
+        return carry
+
+    lax.fori_loop(0, half, far_step, 0)
+    far_copy = remote(att.at[mate_across], am_far, ms.at[1], mr.at[1], {"tp": mate})
+    far_copy.start()
+    w_copy.wait_recv()
+    far_copy.wait_recv()
+    sent = []
+    for c in range(chunks):
+        cols = slice(c * cw, (c + 1) * cw)
+        part = jnp.dot(att[across], w_ref[:, cols], preferred_element_type=f32)
+        part += jnp.dot(am_far[...], w_mate[:, cols], preferred_element_type=f32)
+        ysend[c] = part.astype(bf)
+        copy = remote(ysend.at[c], yrecv.at[c], ys.at[c], yr.at[c], {"tp": across})
+        copy.start()
+        sent.append(copy)
+
+    def near_step(i, carry):
+        attend_block(jnp.where(tp < 2, half - 1 - i, half + i))
+        return carry
+
+    lax.fori_loop(0, half, near_step, 0)
+    near_copy = remote(att.at[mate], am_near, ms.at[2], mr.at[2], {"tp": mate})
+    near_copy.start()
+    near_copy.wait_recv()
+    for c in range(chunks):
+        cols = slice(c * cw, (c + 1) * cw)
+        part = jnp.dot(att[tp], w_ref[:, cols], preferred_element_type=f32)
+        part += jnp.dot(am_near[...], w_mate[:, cols], preferred_element_type=f32)
+        acc[:, cols] = part + res_ref[:, cols].astype(f32)
+    for c in range(chunks):
+        cols = slice(c * cw, (c + 1) * cw)
+        sent[c].wait_recv()
+        out_ref[:, cols] = (acc[:, cols] + yrecv[c].astype(f32)).astype(bf)
+    for copy in halo + [w_copy, far_copy, near_copy] + sent:
+        copy.wait_send()
+
+
+def front(queries, key_rows, value_rows, doc_ids, sink_logit, residual, out_weight):
+    rows, width = residual.shape
+    local, heads_width = queries.shape
+    kv_width = key_rows.shape[1]
+    blocks = local // WINDOW
+    bf, f32 = jnp.bfloat16, jnp.float32
+    dma = pltpu.SemaphoreType.DMA
+    vm = pl.BlockSpec(memory_space=pltpu.VMEM)
+    docs = doc_ids.reshape(blocks, WINDOW)
+    return pl.pallas_call(
+        functools.partial(front_kernel, CHUNKS),
+        out_shape=jax.ShapeDtypeStruct((rows, width), bf),
+        in_specs=[pl.BlockSpec(memory_space=pltpu.SMEM)] + [vm] * 6,
+        out_specs=vm,
+        scratch_shapes=[
+            pltpu.VMEM((blocks + 2, WINDOW, kv_width), bf),
+            pltpu.VMEM((blocks + 2, WINDOW, kv_width), bf),
+            pltpu.VMEM((blocks, WINDOW), jnp.int32),
+            pltpu.VMEM((blocks, WINDOW), jnp.int32),
+            pltpu.VMEM((blocks + 2, 8, WINDOW), f32),
+            pltpu.VMEM((4, rows, heads_width), bf),
+            pltpu.VMEM((rows, heads_width), bf),
+            pltpu.VMEM((rows, heads_width), bf),
+            pltpu.VMEM(out_weight.shape, bf),
+            pltpu.VMEM((rows, width), f32),
+            pltpu.VMEM((CHUNKS, rows, width // CHUNKS), bf),
+            pltpu.VMEM((CHUNKS, rows, width // CHUNKS), bf),
+            dma((6,)), dma((6,)), dma((3,)), dma((3,)), dma((CHUNKS,)), dma((CHUNKS,)),
+        ],
+        compiler_params=pltpu.CompilerParams(
+            collective_id=4, has_side_effects=True, vmem_limit_bytes=48 * 1024 * 1024
+        ),
+        name="front",
+    )(sink_logit, queries, key_rows, value_rows, docs, residual, out_weight)
+
+
 def pair_routed(routes, gate_weight):
     count = lax.axis_size("sp")
     experts = count * gate_weight.shape[0]
@@ -309,22 +488,12 @@
     )(stream, norm_gain[None, :], routes, route_weights, gate_weight, up_weight, down_weight)
 
 
-def per_device(
-    queries,
-    key_rows,
-    value_rows,
-    doc_ids,
-    sink_logit,
-    residual,
-    out_weight,
-    norm_gain,
-    gate_weight,
-    up_weight,
-    down_weight,
-    routes,
-    route_weights,
+def stream_of(
+    queries, key_rows, value_rows, doc_ids, sink_logit, residual, out_weight
 ):
     local_rows = queries.shape[0]
+    if lax.axis_size("tp") == 4 and local_rows % (8 * WINDOW) == 0:
+        return front(queries, key_rows, value_rows, doc_ids, sink_logit, residual, out_weight)
     anchor = lax.axis_index("sp") * local_rows
     extent = local_rows * lax.axis_size("sp")
     doc_float = doc_ids.astype(jnp.bfloat16)
@@ -361,6 +530,27 @@
         )
         running = running + partial_value.astype(jnp.bfloat16).astype(jnp.float32)
     stream = (residual.astype(jnp.float32) + running).astype(jnp.bfloat16)
+    return stream
+
+
+def per_device(
+    queries,
+    key_rows,
+    value_rows,
+    doc_ids,
+    sink_logit,
+    residual,
+    out_weight,
+    norm_gain,
+    gate_weight,
+    up_weight,
+    down_weight,
+    routes,
+    route_weights,
+):
+    stream = stream_of(
+        queries, key_rows, value_rows, doc_ids, sink_logit, residual, out_weight
+    )
     if pair_routed(routes, gate_weight):
         return mixture(
             stream, norm_gain, routes, route_weights, gate_weight, up_weight, down_weight

time: 169 us -> 113 us (0.67)
  Pallas kernels: 67.7 us -> 103 us
  matrix products: 26.9 us -> 0 us
  starting transfers between devices: 22 us -> 0 us
  waiting for transfers between devices: 17.1 us -> 0 us
  other arithmetic: 14.2 us -> 0 us
  between operations: 13.8 us -> 0.06 us
  local copies, waits for them, and re-layouts: 6.83 us -> 9.88 us
    pallas_call x0 -> x1, Pallas kernels: none -> 37.7 us  [front(): pl.pallas_call(functools.partial(front_kernel, CHUNKS), out_shape=jax.Sha...]
    dot_general x8 -> x0, matrix products: 26.9 us -> none  [the longest x2 11.1 us: attend(): jnp.einsum('grqk,kgd->qgrd', attn_weight, value_heads, preferred_element_...]
    ppermute x6 -> x0, starting transfers between devices: 18.3 us -> none  [the longest x3 14.4 us: extended(): lax.ppermute(lax.slice_in_dim(block, block.shape[dim] - width, None, axis...]
    all_to_all x1 -> x0, waiting for transfers between devices: 13.9 us -> none  [per_device(): lax.all_to_all(attended, 'tp', split_axis=0, concat_axis=1, tiled=True)]
    reduce_sum x2 -> x0, other arithmetic: 9.61 us -> none  [attend(): jnp.sum(exponent, axis=3, keepdims=True) + jnp.exp(sink_col - row_top)]
    unnamed x17 -> x21, local copies, waits for them, and re-layouts: 1.28 us -> 9.88 us
    slice x11 -> x0, local copies, waits for them, and re-layouts: 3.87 us -> none  [the longest x3 1.69 us: per_device(): queries[row_start:row_start + block_rows]]
    all_to_all x1 -> x0, starting transfers between devices: 3.7 us -> none  [per_device(): lax.all_to_all(attended, 'tp', split_axis=0, concat_axis=1, tiled=True)]
  transfers between devices with their start and end apart: 8 -> 0, of which waited for: 2 -> 0; matrix products, arithmetic and copies ran while one was open for 24% -> 0% of each run, Pallas kernels for 0% -> 0%
where the time goes in v2:
time: 113 us
  Pallas kernels  103 us (91%)
  local copies, waits for them, and re-layouts  9.88 us (9%)
    pallas_call x1, Pallas kernels, mixture(): pl.pallas_call(functools.partial(moe_kernel, groups, CHUNKS), out_shape=j...  65.4 us
    pallas_call x1, Pallas kernels, front(): pl.pallas_call(functools.partial(front_kernel, CHUNKS), out_shape=jax.Sha...  37.7 us
    unnamed x21, local copies, waits for them, and re-layouts  9.88 us

profile of v2, /device:TPU:0, one launch (start us, length us, event | category | flops | bytes accessed | tf_op | source)
XLA Modules:
  0.0 113.0 jit_solution(6653092205378417138)
XLA Ops:
  0.0 0.8 copy.14.routes_ref
  0.8 0.8 copy.15.rw_ref
  1.6 0.0 copy-start.1
  1.6 1.6 %copy-done.1 = bf16[512,2048]{1,0:T(8,128)(2,1)S(1)} copy-done((bf16[512,2048]{1,0:T(8,128)(2,1)S(1)}, bf16[512,2048]{1,0:T(8,128)(2,1)}, u32[]{:S(2)}) %copy-start.1) | copy-done | bytes 2097176
  3.2 0.0 copy-start.2
  3.2 1.2 %copy-done.2 = bf16[1024,512]{1,0:T(8,128)(2,1)S(1)} copy-done((bf16[1024,512]{1,0:T(8,128)(2,1)S(1)}, bf16[1024,512]{1,0:T(8,128)(2,1)}, u32[]{:S(2)}) %copy-start.2) | copy-done | bytes 1048600
  4.5 0.0 copy-start.3
  4.5 1.2 %copy-done.3 = bf16[256,2048]{1,0:T(8,128)(2,1)S(1)} copy-done((bf16[256,2048]{1,0:T(8,128)(2,1)S(1)}, bf16[256,2048]{1,0:T(8,128)(2,1)}, u32[]{:S(2)}) %copy-start.3) | copy-done | bytes 1048600
  5.7 0.0 copy-start.4
  5.7 0.9 copy-done.4
  6.6 0.0 copy-start.5
  6.6 0.9 copy-done.5
  7.6 0.0 copy-start.7
  7.6 0.7 copy-done.7
  8.3 0.0 copy-start.8
  8.3 0.7 copy-done.8
  8.9 0.0 copy-start
  8.9 0.0 copy-start.6
  8.9 37.7 %front.1.stream_ref = bf16[256,2048]{1,0:T(8,128)(2,1)S(1)} custom-call(f32[8]{0:T(128)S(1)} %copy-done.8, bf16[1024,512]{1,0:T(8,128)(2,1)S(1)} %copy-done.2, bf16[1024,128]{1,0:T(8,128)(2,1)S(1)} %copy-done.4, bf16[1024,128]{1,0:T(8,128)(2,1)S(1)} %copy-done.5, s32[8,128]{1,0:T(8,128)S(1)} %bitcast.3, bf16[256,2048]{1,0:T(8,128)(2,1)S(1)} %copy-done.3, ...), custom_call_target="tpu_custom_call" | custom-call | tf_op jit(solution)/shard_map/front/pallas_call | solution.py:419
  46.6 0.0 copy-done
  46.6 0.0 copy-done.6
  46.6 65.4 %mixture.1 = bf16[256,2048]{1,0:T(8,128)(2,1)S(1)} custom-call(bf16[256,2048]{1,0:T(8,128)(2,1)S(1)} %front.1.stream_ref, f32[1,2048]{1,0:T(1,128)S(1)} %bitcast.2, s32[256,2]{1,0:T(8,128)S(1)} %copy.14.routes_ref, f32[256,2]{1,0:T(8,128)S(1)} %copy.15.rw_ref, bf16[1,2048,512]{2,1,0:T(8,128)(2,1)S(1)} %copy-done, bf16[1,2048,512]{2,1,0:T(8,128)(2,1)} %up_hbm.1, ...), custom_call_target="tpu_custom_call" | custom-call | tf_op jit(solution)/shard_map/mixture/pallas_call | solution.py:467
  112.0 1.0 copy.17
Async XLA Ops:
  1.6 1.6 %copy-start.1 = (bf16[512,2048]{1,0:T(8,128)(2,1)S(1)}, bf16[512,2048]{1,0:T(8,128)(2,1)}, u32[]{:S(2)}) copy-start(bf16[512,2048]{1,0:T(8,128)(2,1)} %w_ref.1) | copy-start | bytes 6291460
  3.2 1.2 %copy-start.2 = (bf16[1024,512]{1,0:T(8,128)(2,1)S(1)}, bf16[1024,512]{1,0:T(8,128)(2,1)}, u32[]{:S(2)}) copy-start(bf16[1024,512]{1,0:T(8,128)(2,1)} %q_ref.1) | copy-start | bytes 3145732
  4.5 1.2 %copy-start.3 = (bf16[256,2048]{1,0:T(8,128)(2,1)S(1)}, bf16[256,2048]{1,0:T(8,128)(2,1)}, u32[]{:S(2)}) copy-start(bf16[256,2048]{1,0:T(8,128)(2,1)} %res_ref.1) | copy-start | bytes 3145732
  5.7 0.9 copy-start.4
  6.6 0.9 copy-start.5
  7.6 0.7 copy-start.7
  8.3 0.7 copy-start.8
  8.9 37.7 %copy-start = (bf16[1,2048,512]{2,1,0:T(8,128)(2,1)S(1)}, bf16[1,2048,512]{2,1,0:T(8,128)(2,1)}, u32[]{:S(2)}) copy-start(bf16[1,2048,512]{2,1,0:T(8,128)(2,1)} %gate_hbm.1) | copy-start | bytes 6291460
  8.9 37.7 %copy-start.6 = (f32[2048]{0:T(1024)S(1)}, f32[2048]{0:T(1024)}, u32[]{:S(2)}) copy-start(f32[2048]{0:T(1024)} %param.20) | copy-start | bytes 24580
